TPU v7x, 32 devices: a whole 2x2x4 slice. The times are simulated.
32 devices in a mesh: grp: 2 (over y), sp: 4 (over z), tp: 4 (over x, core).
Axes of the slice: x: 2, y: 2, z: 4, core: 2. Of those that a mesh axis runs over, the one named last changes fastest.
Arguments:
- latents: bfloat16 [2048, 4, 2048], P(('sp', 'tp'), 'grp'), parts along dimension 1, may hold values from -6 to 6
- context: bfloat16 [1024, 4, 2048], P('sp', 'grp'), parts along dimension 1, may hold values from -6 to 6
- condition: float32 [4, 2048], P('grp', 'sp'), parts along dimension 0, may hold values from -6 to 6
- cond_context: float32 [2048], P('sp'), may hold values from -6 to 6
- w_shift: bfloat16 [2048, 2048], P('sp', 'tp'), may hold values from -0.125 to 0.125
- w_scale: bfloat16 [2048, 2048], P('sp', 'tp'), may hold values from -0.125 to 0.125
- w_gate: bfloat16 [2048, 2048], P('sp', 'tp'), may hold values from -0.375 to 0.375
- norm_gain: float32 [2048], replicated, may hold values from 0.1 to 1.9
- w_query: bfloat16 [2048, 1024], P(None, 'tp'), may hold values from -0.375 to 0.375
- w_key: bfloat16 [2048, 512], P(None, 'tp'), may hold values from -0.125 to 0.125
- w_value: bfloat16 [2048, 512], P(None, 'tp'), may hold values from -0.25 to 0.25
- sink_logit: float32 [16], P('tp'), may hold values from 6 to 240
- w_out: bfloat16 [1024, 2048], P('tp'), may hold values from -0.1875 to 0.1875
Outputs:
- refined: bfloat16 [2048, 4, 2048], P(('sp', 'tp'), 'grp'), parts along dimension 1
There are 2 independent parts, one for each index of `grp`. A program takes and returns all parts, laid end to end along the dimension named above; an argument that names none is the same for every part. Nothing has to cross between parts.
All inputs are finite; a program needn't handle non-finite values.
Results may differ from a plain program's by a relative error of at most 0.017.
Values may be sent and summed in bfloat16 or wider, within the bound.
No kernel may reach another device: no remote copies, remote signals or barrier semaphores. Data moves between devices by JAX's collectives and lax.ppermute only.
A program may use at most 128 MiB of HBM per device.

v0:
```python
import jax
import jax.numpy as jnp
from jax import lax
from jax.sharding import PartitionSpec as P

HEAD_DIM = 64
WINDOW = 128
GRID_W = 64
EPS = 1e-06
THETA = 10000.0
BIG_NEG = -1e30


def with_halo(cells, sides, width):
    for axis, dim in sides:
        count = lax.axis_size(axis)
        ends = count - 1
        head = lax.slice_in_dim(cells, 0, width, axis=dim)
        tail = lax.slice_in_dim(cells, cells.shape[dim] - width, cells.shape[dim], axis=dim)
        cells = jnp.concatenate(
            [
                lax.ppermute(tail, axis, [(i, (i + 1) % count) for i in range(ends)]),
                cells,
                lax.ppermute(head, axis, [((i + 1) % count, i) for i in range(ends)]),
            ],
            axis=dim,
        )
    return cells


def rotate_pairs(vectors, grid_row, grid_col, head_dim):
    quarter = head_dim // 4
    inverse = THETA ** (-jnp.arange(quarter, dtype=jnp.float32) / quarter)
    angles = jnp.concatenate([grid_row[:, None] * inverse, grid_col[:, None] * inverse], axis=-1)
    shape = (angles.shape[0],) + (1,) * (vectors.ndim - 2) + (head_dim // 2,)
    cosine = jnp.cos(angles).reshape(shape)
    sine = jnp.sin(angles).reshape(shape)
    first_half = vectors[..., : head_dim // 2]
    second_half = vectors[..., head_dim // 2 :]
    return jnp.concatenate(
        [first_half * cosine - second_half * sine, first_half * sine + second_half * cosine],
        axis=-1,
    )


def modulate(tokens_in, gain, shift_rows, scale_rows):
    upcast = tokens_in.astype(jnp.float32)
    normed = upcast * lax.rsqrt(jnp.mean(upcast * upcast, axis=-1, keepdims=True) + EPS)
    return (normed * gain * (1.0 + scale_rows) + shift_rows).astype(jnp.bfloat16)


def on_device(
    latents,
    context,
    condition,
    cond_context,
    w_shift,
    w_scale,
    w_gate,
    norm_gain,
    w_query,
    w_key,
    w_value,
    sink_logit,
    w_out,
):
    samples = latents.shape[1]
    model_width = latents.shape[2]
    n_tp = lax.axis_size("tp")
    n_sp = lax.axis_size("sp")
    local_rows = latents.shape[0]
    tokens = local_rows * n_tp
    local_heads = w_query.shape[1] // HEAD_DIM
    local_kv = w_key.shape[1] // HEAD_DIM
    per_group = local_heads // local_kv
    q_cols = local_heads * HEAD_DIM
    kv_cols = local_kv * HEAD_DIM
    lifted = jax.nn.silu(jnp.concatenate([condition, cond_context[None, :]], axis=0)).astype(
        jnp.bfloat16
    )
    part_shift = jnp.dot(lifted, w_shift, preferred_element_type=jnp.float32)
    part_scale = jnp.dot(lifted, w_scale, preferred_element_type=jnp.float32)
    part_gate = jnp.dot(lifted, w_gate, preferred_element_type=jnp.float32)
    sum_shift, sum_scale, sum_gate = lax.psum((part_shift, part_scale, part_gate), "sp")
    shift_all, scale_all, gate_all = (
        lax.all_gather(sum_shift, "tp", axis=1, tiled=True),
        lax.all_gather(sum_scale, "tp", axis=1, tiled=True),
        lax.all_gather(sum_gate, "tp", axis=1, tiled=True),
    )
    normed = modulate(latents, norm_gain, shift_all[:samples][None], scale_all[:samples][None])
    w_joint = jnp.concatenate([w_query, w_key, w_value], axis=1)
    shard_rows = lax.all_gather(normed, "tp", axis=0, tiled=True)
    row_count = shard_rows.shape[0]
    flat_rows = shard_rows.reshape(row_count * samples, model_width)
    projected = jnp.dot(flat_rows, w_joint, preferred_element_type=jnp.float32).reshape(
        row_count, samples, w_joint.shape[1]
    )
    offset = lax.axis_index("sp") * tokens
    positions = offset + jnp.arange(tokens, dtype=jnp.int32)
    grid_row = (positions // GRID_W).astype(jnp.float32)
    grid_col = (positions % GRID_W).astype(jnp.float32)
    queries = rotate_pairs(
        projected[..., :q_cols].reshape(tokens, samples, local_heads, HEAD_DIM),
        grid_row,
        grid_col,
        HEAD_DIM,
    ).astype(jnp.bfloat16)
    lat_keys = rotate_pairs(
        projected[..., q_cols : q_cols + kv_cols].reshape(tokens, samples, local_kv, HEAD_DIM),
        grid_row,
        grid_col,
        HEAD_DIM,
    ).astype(jnp.bfloat16)
    lat_values = projected[..., q_cols + kv_cols :].astype(jnp.bfloat16)
    paired = jnp.concatenate([lat_keys.reshape(tokens, samples, kv_cols), lat_values], axis=-1)
    extended = with_halo(paired, (("sp", 0),), WINDOW)
    w_pair = jnp.concatenate([w_key, w_value], axis=1)
    ctx_shift = shift_all[samples][None, None]
    ctx_scale = scale_all[samples][None, None]
    ctx_normed = modulate(context, norm_gain, ctx_shift, ctx_scale)
    row_count = context.shape[0]
    flat_ctx = ctx_normed.reshape(row_count * samples, model_width)
    ctx_pairs = lax.all_gather(
        jnp.dot(flat_ctx, w_pair, preferred_element_type=jnp.float32)
        .astype(jnp.bfloat16)
        .reshape(row_count, samples, 2 * kv_cols),
        "sp",
        axis=0,
        tiled=True,
    )
    ctx_len = ctx_pairs.shape[0]
    ctx_keys = ctx_pairs[..., :kv_cols].reshape(ctx_len, samples, local_kv, HEAD_DIM)
    ctx_values = ctx_pairs[..., kv_cols:].reshape(ctx_len, samples, local_kv, HEAD_DIM)
    block_rows = min(tokens, 512)
    n_blocks = tokens // block_rows
    seq_length = tokens * n_sp
    head_sinks = sink_logit.reshape(local_kv, per_group)[None, :, :, None]
    score_scale = HEAD_DIM ** (-0.5)

    def attend_block(block_index):
        first_row = block_index * block_rows
        q_blk = queries.reshape(block_rows, samples, local_kv, per_group, HEAD_DIM)
        k_blk = extended[..., :kv_cols].reshape(
            block_rows + 2 * WINDOW, samples, local_kv, HEAD_DIM
        )
        v_blk = extended[..., kv_cols:].reshape(
            block_rows + 2 * WINDOW, samples, local_kv, HEAD_DIM
        )
        lat_scores = (
            jnp.einsum("qsngd,ksnd->sngqk", q_blk, k_blk, preferred_element_type=jnp.float32)
            * score_scale
        )
        q_pos = offset + first_row + jnp.arange(block_rows, dtype=jnp.int32)
        k_pos = offset + first_row - WINDOW + jnp.arange(block_rows + 2 * WINDOW, dtype=jnp.int32)
        in_window = (
            (jnp.abs(q_pos[:, None] - k_pos[None, :]) <= WINDOW)
            & (k_pos >= 0)[None, :]
            & (k_pos < seq_length)[None, :]
        )
        lat_scores = jnp.where(in_window, lat_scores, BIG_NEG)
        ctx_scores = (
            jnp.einsum("qsngd,ksnd->sngqk", q_blk, ctx_keys, preferred_element_type=jnp.float32)
            * score_scale
        )
        row_max = jnp.maximum(
            jnp.maximum(jnp.max(lat_scores, axis=-1), jnp.max(ctx_scores, axis=-1)), head_sinks
        )
        lat_exp = jnp.exp(lat_scores - row_max[..., None])
        ctx_exp = jnp.exp(ctx_scores - row_max[..., None])
        denominator = (
            jnp.sum(lat_exp, axis=-1) + jnp.sum(ctx_exp, axis=-1) + jnp.exp(head_sinks - row_max)
        )
        lat_weights = (lat_exp / denominator[..., None]).astype(jnp.bfloat16)
        ctx_weights = (ctx_exp / denominator[..., None]).astype(jnp.bfloat16)
        summed = jnp.einsum(
            "sngqk,ksnd->qsngd", lat_weights, v_blk, preferred_element_type=jnp.float32
        )
        summed = summed + jnp.einsum(
            "sngqk,ksnd->qsngd", ctx_weights, ctx_values, preferred_element_type=jnp.float32
        )
        return summed.astype(jnp.bfloat16).reshape(block_rows, samples, q_cols)

    attended = lax.map(attend_block, jnp.arange(n_blocks)).reshape(tokens * samples, q_cols)
    summed_out = lax.psum_scatter(
        jnp.dot(attended, w_out, preferred_element_type=jnp.float32).astype(jnp.bfloat16),
        "tp",
        scatter_dimension=0,
        tiled=True,
    ).astype(jnp.float32)
    mixed = summed_out.reshape(local_rows, samples, model_width)
    refined = latents.astype(jnp.float32) + gate_all[:samples][None] * mixed
    return refined.astype(jnp.bfloat16)


def solution(mesh):
    return jax.shard_map(
        on_device,
        mesh=mesh,
        in_specs=(
            P(("sp", "tp"), "grp", None),
            P("sp", "grp", None),
            P("grp", "sp"),
            P("sp"),
            P("sp", "tp"),
            P("sp", "tp"),
            P("sp", "tp"),
            P(),
            P(None, "tp"),
            P(None, "tp"),
            P(None, "tp"),
            P("tp"),
            P("tp", None),
        ),
        out_specs=P(("sp", "tp"), "grp", None),
        check_vma=False,
    )
```

profile of v0, /device:TPU:0, one launch (start us, length us, event | category | flops | bytes accessed | tf_op | source)
XLA Modules:
  0.0 237.9 jit_solution(7936242793611745387)
XLA Ops:
  6.5 0.0 copy-start
  6.5 1.4 fusion.49
  7.9 1.3 fusion.51
  9.2 1.3 fusion.53
  10.5 20.7 %all-reduce = (f32[3,512]{1,0:T(4,128)S(1)}, f32[3,512]{1,0:T(4,128)S(1)}, f32[3,512]{1,0:T(4,128)S(1)}) all-reduce(f32[3,512]{1,0:T(4,128)S(1)} %fusion.49, f32[3,512]{1,0:T(4,128)S(1)} %fusion.51, f32[3,512]{1,0:T(4,128)S(1)} %fusion.53), channel_id=1, replica_groups=mesh['grp'=2,'sp'=4,'tp'=4] {'sp'}, use_global_device_ids=true, to_apply=%region_3.4 | all-reduce | flops 4608 | bytes 36864 | tf_op jit(solution)/shard_map/psum | solution.py:84
  31.1 5.2 %all_gather.17 = f32[3,2048]{1,0:T(4,128)S(1)} all-gather(f32[3,512]{1,0:T(4,128)S(1)} %get-tuple-element.19), channel_id=1, replica_groups=mesh['grp'=2,'sp'=4,'tp'=4] {'tp'}, dimensions={1}, use_global_device_ids=true | all-gather | bytes 30720 | tf_op jit(solution)/shard_map/all_gather | solution.py:86
  36.3 5.2 %all_gather.16 = f32[3,2048]{1,0:T(4,128)S(1)} all-gather(f32[3,512]{1,0:T(4,128)S(1)} %get-tuple-element.20), channel_id=1, replica_groups=mesh['grp'=2,'sp'=4,'tp'=4] {'tp'}, dimensions={1}, use_global_device_ids=true | all-gather | bytes 30720 | tf_op jit(solution)/shard_map/all_gather | solution.py:87
  41.5 3.8 %fusion.6 = f32[256,2]{1,0:T(8,128)S(1)} fusion(bf16[256,2,2048]{2,1,0:T(2,128)(2,1)} %param.14), kind=kLoop, calls=%fused_computation.14 | loop fusion | flops 3145216 | bytes 2099200 | tf_op jit(solution)/shard_map/reduce_sum | solution.py:48
  45.4 4.5 %fusion.10 = bf16[256,2,2048]{2,1,0:T(2,128)(2,1)} fusion(bf16[256,2,2048]{2,1,0:T(2,128)(2,1)S(1)} %copy-done.3, f32[2048]{0:T(1024)S(1)} %bitcast.83, f32[2048]{0:T(1024)S(1)} %bitcast.84, f32[2048]{0:T(1024)S(1)} %copy-done.6, f32[256,2]{1,0:T(8,128)S(1)} %add_rsqrt_fusion), kind=kLoop, calls=%fused_computation.18 | loop fusion | flops 6291456 | bytes 4220928 | tf_op jit(solution)/shard_map/convert_element_type | solution.py:49
  50.0 4.2 %reshape.218 = bf16[512,2048]{1,0:T(8,128)(2,1)} reshape(bf16[256,2,2048]{2,1,0:T(2,128)(2,1)} %fusion.10) | data formatting | bytes 4194304 | tf_op jit(solution)/shard_map/reshape | solution.py:122
  54.2 2.4 %convolution_convert_fusion.1 = bf16[512,256]{1,0:T(8,128)(2,1)S(1)} fusion(bf16[512,2048]{1,0:T(8,128)(2,1)} %reshape.218, bf16[2048,128]{1,0:T(8,128)(2,1)S(1)} %copy-done.4, bf16[2048,128]{1,0:T(8,128)(2,1)} %param.22), kind=kOutput, calls=%fused_computation.42 | convolution fusion | flops 539099136 | bytes 3407872 | tf_op jit(solution)/shard_map/dot_general | solution.py:124
  56.6 0.8 reshape.219
  57.4 0.0 all-gather.5.cloned.1.call-update
  57.4 0.0 all-gather.3.cloned.1.call-start
  57.5 0.0 copy-done.2
  57.5 0.0 copy-start.8
  57.5 0.4 fusion.11
  57.9 1.6 fusion.15
  59.5 0.0 all-gather.3.cloned.1.call-update
  59.5 0.0 reduce-scatter.2.cloned.1.call-start
  59.6 1.0 copy.60
  60.6 2.0 copy.59
  62.6 2.3 copy.58
  64.9 0.1 max.33
  65.1 0.1 broadcast_multiply_fusion.1
  65.1 0.2 fusion.33
  65.4 0.8 fusion.23
  66.2 17.6 %all-gather.5.cloned.1.call-done = bf16[1024,2,256]{2,1,0:T(2,128)(2,1)} async-done(((bf16[256,2,256]{2,1,0:T(2,128)(2,1)}), bf16[1024,2,256]{2,1,0:T(2,128)(2,1)}) %all-gather.5.cloned.1.call-update) | async-done | bytes 1048592 | tf_op jit(solution)/shard_map/all_gather | solution.py:123
  83.8 2.7 %fusion.55 = (bf16[1024,2,128]{2,1,0:T(2,128)(2,1)}, bf16[1024,2,128]{2,1,0:T(2,128)(2,1)S(1)}) fusion(bf16[1024,2,256]{2,1,0:T(2,128)(2,1)} %all-gather.5.cloned.1.call-done), kind=kLoop, calls=%fused_computation.98 | loop fusion | bytes 2097152 | tf_op jit(solution)/shard_map/slice | solution.py:132
  86.5 1.1 copy.65
  87.6 1.3 copy.63
  88.9 30.3 %all-gather.3.cloned.1.call-done = bf16[512,2,2048]{2,0,1:T(8,128)(2,1)} async-done(((bf16[128,2,2048]{2,0,1:T(8,128)(2,1)}), bf16[512,2,2048]{2,0,1:T(8,128)(2,1)}) %all-gather.3.cloned.1.call-update) | async-done | bytes 4194320 | tf_op jit(solution)/shard_map/all_gather | solution.py:92
  119.2 5.2 %fusion.17 = f32[512,2,512]{0,2,1:T(8,128)S(1)} fusion(bf16[512,2,2048]{2,0,1:T(8,128)(2,1)} %all-gather.3.cloned.1.call-done, bf16[2048,128]{0,1:T(8,128)(2,1)} %copy.60, bf16[2048,128]{0,1:T(8,128)(2,1)} %copy.59, bf16[2048,256]{0,1:T(8,128)(2,1)} %copy.58), kind=kOutput, calls=%fused_computation.30 | convolution fusion | flops 2153775104 | bytes 8388608 | tf_op jit(solution)/shard_map/dot_general | solution.py:95
  124.4 0.1 slice.84
  124.5 0.2 subtract_convert_fusion
  124.7 0.1 subtract_convert_fusion.1
  124.9 1.3 collective-permute-start.1
  126.2 4.7 %collective-permute-start = (bf16[128,2,256]{0,2,1:T(8,128)(2,1)S(1)}, bf16[128,2,256]{0,2,1:T(8,128)(2,1)S(1)}, u32[]{:S(2)}, u32[]{:S(2)}) collective-permute-start(bf16[128,2,256]{0,2,1:T(8,128)(2,1)S(1)} %get-tuple-element.40), channel_id=1, source_target_pairs={{0,4},{4,8},{8,12},{1,5},{5,9},{9,13},{2,6},{6,10},{10,14},{3,7},{... | collective-permute-start | bytes 393224 | tf_op jit(solution)/shard_map/ppermute | solution.py:22
  130.9 8.1 %bitcast_reduce_fusion = (f32[2,2,2,512]{3,2,1,0:T(2,128)S(1)}, f32[2,2,1024,512,2]{3,2,4,1,0:T(8,128)}) fusion(bf16[1024,2,2,64,1]{0,3,4,2,1:T(8,128)(2,1)S(1)} %bitcast.74, bf16[512,2,2,2,32]{0,4,3,2,1:T(8,128)(2,1)S(1)} %bitcast.78, bf16[512,2,2,2,32]{0,4,3,2,1:T(8,128)(2,1)S(1)} %bitcast.76), kind=kOutput, calls=%fused_computation.1 | convolution fusion | flops 546304000 | bytes 17842176 | tf_op jit(solution)/shard_map/while/body/eval_jaxpr/qsngd,ksnd->sngqk/dot_general | solution.py:162
  139.0 0.0 collective-permute-done.1
  139.0 0.0 collective-permute-done
  139.1 0.1 pad_maximum_fusion
  139.1 0.8 fusion.56
  139.9 2.1 fusion.3
  142.1 0.1 maximum_maximum_fusion
  142.2 2.6 %fusion.2 = f32[2,2,2,512]{3,2,1,0:T(2,128)S(1)} fusion(f32[2,2,768,512,2]{3,2,4,1,0:T(8,128)S(1)} %get-tuple-element.47, f32[2,2,2,512]{3,2,1,0:T(2,128)S(1)} %maximum_maximum_fusion, pred[512,768]{0,1:T(8,128)(4,1)S(1)} %fusion.23), kind=kLoop, calls=%fused_computation.8 | loop fusion | flops 12578816 | bytes 13008896 | tf_op jit(solution)/shard_map/while/body/eval_jaxpr/reduce_sum | solution.py:171
  144.8 1.8 copy-done.1
  146.6 9.3 %fusion.1 = f32[2,2,2,512]{3,2,1,0:T(2,128)} fusion(f32[2,2,1024,512,2]{3,2,4,1,0:T(8,128)} %get-tuple-element.49, f32[2,2,2,512]{3,2,1,0:T(2,128)S(1)} %maximum_maximum_fusion), kind=kLoop, calls=%fused_computation.4 | loop fusion | flops 12578816 | bytes 16809984 | tf_op jit(solution)/shard_map/while/body/eval_jaxpr/reduce_sum | solution.py:171
  155.9 0.8 exponential_add_fusion
  156.7 0.0 slice-start.1
  156.8 0.0 slice-start.2
  156.8 0.0 copy-start.5
  156.8 8.0 %fusion.4 = f32[2,2,64,2,512]{4,2,3,1,0:T(8,128)S(1)} fusion(bf16[1024,2,2,64,1]{0,3,4,2,1:T(8,128)(2,1)} %bitcast.80, f32[2,2,1024,512,2]{3,2,4,1,0:T(8,128)} %get-tuple-element.49, f32[2,2,2,512]{3,2,1,0:T(2,128)S(1)} %exponential_add_fusion, f32[2,2,2,512]{3,2,1,0:T(2,128)S(1)} %maximum_maximum_fusion), kind=kOutput, calls=%fused_computation.10 | convolution fusion | flops 553648128 | bytes 18382848 | tf_op jit(solution)/shard_map/while/body/eval_jaxpr/sngqk,ksnd->qsngd/dot_general | solution.py:178
  164.8 0.4 slice-done.2
  165.3 4.3 %fusion.26 = bf16[512,2,2,2,64]{0,4,3,2,1:T(8,128)(2,1)} fusion(f32[2,2,64,2,512]{4,2,3,1,0:T(8,128)S(1)} %fusion.4, bf16[768,2,2,64,1]{0,3,4,2,1:T(8,128)(2,1)S(1)} %bitcast.81, f32[2,2,768,512,2]{3,2,4,1,0:T(8,128)S(1)} %bitcast.70, f32[2,2,2,512]{3,2,1,0:T(2,128)S(1)} %exponential_add_fusion, f32[2,2,2,512]{3,2,1,0:T(2,128)S(1)} %maximum_maximum_fusion, ...), kind=kOutput, calls=%fused_computation.41 | convolution fusion | flops 418906112 | bytes 14974976 | tf_op jit(solution)/shard_map/while/body/eval_jaxpr/sngqk,ksnd->qsngd/dot_general | solution.py:175
  169.6 3.6 %copy.67 = bf16[512,2,2,2,64]{4,3,2,1,0:T(2,128)(2,1)} copy(bf16[512,2,2,2,64]{0,4,3,2,1:T(8,128)(2,1)} %fusion.26) | data formatting | bytes 1048576 | tf_op jit(solution)/shard_map/while/body/eval_jaxpr/convert_element_type | solution.py:181
  173.1 2.8 %reshape.222 = bf16[1024,256]{1,0:T(8,128)(2,1)S(1)} reshape(bf16[512,2,2,2,64]{4,3,2,1,0:T(2,128)(2,1)} %copy.67) | data formatting | bytes 1048576 | tf_op jit(solution)/shard_map/reshape | solution.py:183
  175.9 3.2 %convolution_convert_fusion = bf16[1024,2048]{1,0:T(8,128)(2,1)} fusion(bf16[1024,256]{1,0:T(8,128)(2,1)S(1)} %reshape.222, bf16[256,2048]{1,0:T(8,128)(2,1)S(1)} %copy-done), kind=kOutput, calls=%fused_computation.19 | convolution fusion | flops 1075838976 | bytes 5767168 | tf_op jit(solution)/shard_map/dot_general | solution.py:185
  179.1 0.0 reduce-scatter.2.cloned.1.call-update
  179.1 5.2 %all_gather.15 = f32[3,2048]{1,0:T(4,128)S(1)} all-gather(f32[3,512]{1,0:T(4,128)S(1)} %get-tuple-element.21), channel_id=1, replica_groups=mesh['grp'=2,'sp'=4,'tp'=4] {'tp'}, dimensions={1}, use_global_device_ids=true | all-gather | bytes 30720 | tf_op jit(solution)/shard_map/all_gather | solution.py:88
  184.3 38.6 %reduce-scatter.2.cloned.1.call-done = bf16[256,2048]{1,0:T(8,128)(2,1)} async-done(((bf16[1024,2048]{1,0:T(8,128)(2,1)}), bf16[256,2048]{1,0:T(8,128)(2,1)}) %reduce-scatter.2.cloned.1.call-update) | async-done | bytes 1048592 | tf_op jit(solution)/shard_map/reduce_scatter | solution.py:184
  223.0 3.4 %reshape.226 = f32[128,2,2048]{2,1,0:T(2,128)} reshape(bf16[256,2048]{1,0:T(8,128)(2,1)} %reduce-scatter.2.cloned.1.call-done) | data formatting | bytes 3145728 | tf_op jit(solution)/shard_map/reshape | solution.py:190
  226.3 3.0 %fusion.16 = bf16[128,2,2048]{2,0,1:T(8,128)(2,1)S(1)} fusion(f32[128,2,2048]{2,1,0:T(2,128)} %reshape.226, f32[2,2048]{1,0:T(2,128)S(1)} %slice.75, bf16[128,2,2048]{2,1,0:T(2,128)(2,1)S(1)} %copy-done.2), kind=kLoop, calls=%fused_computation.28 | loop fusion | flops 2097152 | bytes 4210688 | tf_op jit(solution)/shard_map/convert_element_type | solution.py:192
  229.3 2.0 copy.69
  (34 shorter events, 0.3 us)
Async XLA Ops:
  6.5 169.3 %copy-start = (bf16[256,2048]{1,0:T(8,128)(2,1)S(1)}, bf16[256,2048]{1,0:T(8,128)(2,1)}, u32[]{:S(2)}) copy-start(bf16[256,2048]{1,0:T(8,128)(2,1)} %param.25) | copy-start | bytes 3145732
  6.5 38.9 %copy-start.3 = (bf16[256,2,2048]{2,1,0:T(2,128)(2,1)S(1)}, bf16[256,2,2048]{2,1,0:T(2,128)(2,1)}, u32[]{:S(2)}) copy-start(bf16[256,2,2048]{2,1,0:T(2,128)(2,1)} %param.14) | copy-start | bytes 6291460
  6.5 38.9 %copy-start.6 = (f32[2048]{0:T(1024)S(1)}, f32[2048]{0:T(1024)}, u32[]{:S(2)}) copy-start(f32[2048]{0:T(1024)} %param.20) | copy-start | bytes 24580
  6.5 77.2 %all-gather.5.cloned.1.call-start = ((), (), s32[]{:S(2)}) async-start(), calls=%async_computation.2 | async-start | bytes 1310720 | tf_op jit(solution)/shard_map/all_gather | solution.py:123
  50.0 4.2 %copy-start.4 = (bf16[2048,128]{1,0:T(8,128)(2,1)S(1)}, bf16[2048,128]{1,0:T(8,128)(2,1)}, u32[]{:S(2)}) copy-start(bf16[2048,128]{1,0:T(8,128)(2,1)} %param.23) | copy-start | bytes 1572868
  50.0 7.5 %copy-start.2 = (bf16[128,2,2048]{2,1,0:T(2,128)(2,1)S(1)}, bf16[128,2,2048]{2,1,0:T(2,128)(2,1)}, u32[]{:S(2)}) copy-start(bf16[128,2,2048]{2,1,0:T(2,128)(2,1)} %param.13) | copy-start | bytes 3145732
  57.4 61.8 %all-gather.3.cloned.1.call-start = ((), (), s32[]{:S(2)}) async-start(), calls=%async_computation.1 | async-start | bytes 5242880 | tf_op jit(solution)/shard_map/all_gather | solution.py:92
  57.5 7.4 %copy-start.8 = (f32[4]{0:T(128)S(1)}, f32[4]{0:T(128)}, u32[]{:S(2)}) copy-start(f32[4]{0:T(128)} %param.24) | copy-start | bytes 52
  59.5 163.5 %reduce-scatter.2.cloned.1.call-start = ((), (), s32[]{:S(2)}) async-start(), calls=%async_computation.3 | async-start | bytes 5242880 | tf_op jit(solution)/shard_map/reduce_scatter | solution.py:184
  65.0 77.1 %copy-start.7 = (f32[2,2]{1,0:T(2,128)}, f32[2,2]{1,0:T(2,128)S(1)}, u32[]{:S(2)}) copy-start(f32[2,2]{1,0:T(2,128)S(1)} %max.33) | copy-start | bytes 52
  124.9 14.2 %collective-permute-start.1 = (bf16[128,2,256]{0,2,1:T(8,128)(2,1)S(1)}, bf16[128,2,256]{0,2,1:T(8,128)(2,1)S(1)}, u32[]{:S(2)}, u32[]{:S(2)}) collective-permute-start(bf16[128,2,256]{0,2,1:T(8,128)(2,1)S(1)} %get-tuple-element.41), channel_id=1, source_target_pairs={{4,0},{8,4},{12,8},{5,1},{9,5},{13,9},{6,2},{10,6},{14,10},{7,3},{... | collective-permute-start | bytes 393224 | tf_op jit(solution)/shard_map/ppermute | solution.py:24
  126.2 12.9 %collective-permute-start = (bf16[128,2,256]{0,2,1:T(8,128)(2,1)S(1)}, bf16[128,2,256]{0,2,1:T(8,128)(2,1)S(1)}, u32[]{:S(2)}, u32[]{:S(2)}) collective-permute-start(bf16[128,2,256]{0,2,1:T(8,128)(2,1)S(1)} %get-tuple-element.40), channel_id=1, source_target_pairs={{0,4},{4,8},{8,12},{1,5},{5,9},{9,13},{2,6},{6,10},{10,14},{3,7},{... | collective-permute-start | bytes 393224 | tf_op jit(solution)/shard_map/ppermute | solution.py:22
  142.1 4.5 %copy-start.1 = (f32[2,2,768,512,2]{3,2,4,1,0:T(8,128)}, f32[2,2,768,512,2]{3,2,4,1,0:T(8,128)S(1)}, u32[]{:S(2)}) copy-start(f32[2,2,768,512,2]{3,2,4,1,0:T(8,128)S(1)} %get-tuple-element.47) | copy-start | bytes 37748740
  146.6 18.2 %slice-start = ((s8[12582912]{0:T(1024)(128)(4,1)}), s8[4194304]{0:T(1024)(128)(4,1)S(1)}, s32[]{:S(2)}) async-start(s8[12582912]{0:T(1024)(128)(4,1)} %bitcast.69), calls=%async_computation.4 | async-start | bytes 8388608
  156.7 8.1 %slice-start.1 = ((s8[12582912]{0:T(1024)(128)(4,1)}), s8[4194304]{0:T(1024)(128)(4,1)S(1)}, s32[]{:S(2)}) async-start(s8[12582912]{0:T(1024)(128)(4,1)} %bitcast.69), calls=%async_computation.5 | async-start | bytes 8388608
  156.8 8.5 %slice-start.2 = ((s8[12582912]{0:T(1024)(128)(4,1)}), s8[4194304]{0:T(1024)(128)(4,1)S(1)}, s32[]{:S(2)}) async-start(s8[12582912]{0:T(1024)(128)(4,1)} %bitcast.69), calls=%async_computation.6 | async-start | bytes 8388608
  156.8 8.5 %copy-start.5 = (bf16[768,2,128]{0,2,1:T(8,128)(2,1)S(1)}, bf16[768,2,128]{0,2,1:T(8,128)(2,1)}, u32[]{:S(2)}) copy-start(bf16[768,2,128]{0,2,1:T(8,128)(2,1)} %get-tuple-element.36) | copy-start | bytes 1179652
Sparse Core Ops, SparseCore 0:
  57.5 26.2 all-gather.4
  85.3 33.8 all-gather.2
  179.2 43.6 reduce-scatter.1
where the time goes:
time: 239 us; the launch traced here: 238 us
  waiting for transfers between devices  86.6 us (36%)
  matrix products  37.3 us (16%)
  blocking collectives  36.2 us (15%)
  local copies, waits for them, and re-layouts  30.6 us (13%)
  other arithmetic  27.7 us (12%)
  between operations  13.4 us (6%)
  starting transfers between devices  6.11 us (3%)
    reduce_scatter x1, waiting for transfers between devices, on_device(): lax.psum_scatter(jnp.dot(attended, w_out, preferred_element_type=jnp.floa...  38.6 us
    all_gather x1, waiting for transfers between devices, on_device(): shard_rows = lax.all_gather(normed, 'tp', axis=0, tiled=True)  30.3 us
    psum x1, blocking collectives, on_device(): lax.psum((part_shift, part_scale, part_gate), 'sp')  20.7 us
    all_gather x1, waiting for transfers between devices, on_device(): lax.all_gather(jnp.dot(flat_ctx, w_pair, preferred_element_type=jnp.float...  17.6 us
    reduce_sum x1, other arithmetic, attend_block(): jnp.sum(ctx_exp, axis=-1)  9.31 us
    dot_general x1, matrix products, attend_block(): jnp.einsum('qsngd,ksnd->sngqk', q_blk, ctx_keys, preferred_element_type=j...  8.13 us
    dot_general x1, matrix products, attend_block(): jnp.einsum('sngqk,ksnd->qsngd', ctx_weights, ctx_values, preferred_elemen...  8.03 us
    unnamed x27, local copies, waits for them, and re-layouts  7.63 us
  transfers between devices with their start and end apart: 5, of which 3 were waited for; matrix products, arithmetic and copies ran while one was open for 9% of the time, Pallas kernels for 0%

commit v1 on v0

--- a/solution.py
+++ b/solution.py
@@ -9,6 +9,22 @@
 EPS = 1e-06
 THETA = 10000.0
 BIG_NEG = -1e30
+
+
+def start_the_stages_all(raw):
+    nd = lax.psum(1, "tp")
+    pool = [(it, (it + 1) % nd) for it in range(nd)]
+
+    def hubs_find(w2):
+        if len(w2) == nd:
+            return w2
+        m_next = lax.ppermute(w2[0], "tp", pool)
+        return hubs_find([m_next, *w2])
+
+    placed = hubs_find([raw])
+    later = jnp.concatenate(placed, axis=0)
+    passed = lax.axis_index("tp")
+    return jnp.roll(later, (passed + 1) * raw.shape[0], axis=0)
 
 
 def with_halo(cells, sides, width):
@@ -89,7 +105,7 @@
     )
     normed = modulate(latents, norm_gain, shift_all[:samples][None], scale_all[:samples][None])
     w_joint = jnp.concatenate([w_query, w_key, w_value], axis=1)
-    shard_rows = lax.all_gather(normed, "tp", axis=0, tiled=True)
+    shard_rows = start_the_stages_all(normed)
     row_count = shard_rows.shape[0]
     flat_rows = shard_rows.reshape(row_count * samples, model_width)
     projected = jnp.dot(flat_rows, w_joint, preferred_element_type=jnp.float32).reshape(

time: 239 us -> 220 us (0.921)
  waiting for transfers between devices: 86.6 us -> 60.8 us
  local copies, waits for them, and re-layouts: 30.6 us -> 36.3 us
    all_gather x1 -> x0, waiting for transfers between devices: 30.3 us -> none  [on_device(): shard_rows = lax.all_gather(normed, 'tp', axis=0, tiled=True)]
    ppermute x0 -> x3, waiting for transfers between devices: none -> 8.06 us  [hubs_find(): m_next = lax.ppermute(w2[0], 'tp', pool)]
    unnamed x27 -> x53, local copies, waits for them, and re-layouts: 7.63 us -> 14.3 us
    all_gather x1, waiting for transfers between devices: 17.6 us -> 13.8 us  [on_device(): lax.all_gather(jnp.dot(flat_ctx, w_pair, preferred_element_type=jnp.float...]
    dot_general x1, matrix products: 5.16 us -> 2.39 us  [on_device(): jnp.dot(flat_rows, w_joint, preferred_element_type=jnp.float32)]
  transfers between devices with their start and end apart: 5 -> 7, of which waited for: 3 -> 4; matrix products, arithmetic and copies ran while one was open for 9% -> 17% of each run, Pallas kernels for 0% -> 0%
where the time goes in v1:
time: 220 us; the launch traced here: 219 us
  waiting for transfers between devices  60.8 us (28%)
  blocking collectives  36.8 us (17%)
  local copies, waits for them, and re-layouts  36.3 us (16%)
  matrix products  35.7 us (16%)
  other arithmetic  29 us (13%)
  between operations  13.9 us (6%)
  starting transfers between devices  6.47 us (3%)
    reduce_scatter x1, waiting for transfers between devices, on_device(): lax.psum_scatter(jnp.dot(attended, w_out, preferred_element_type=jnp.floa...  38.9 us
    psum x1, blocking collectives, on_device(): lax.psum((part_shift, part_scale, part_gate), 'sp')  21.3 us
    unnamed x53, local copies, waits for them, and re-layouts  14.3 us
    all_gather x1, waiting for transfers between devices, on_device(): lax.all_gather(jnp.dot(flat_ctx, w_pair, preferred_element_type=jnp.float...  13.8 us
    reduce_sum x1, other arithmetic, attend_block(): jnp.sum(ctx_exp, axis=-1)  8.61 us
    dot_general x1, matrix products, attend_block(): jnp.einsum('qsngd,ksnd->sngqk', q_blk, ctx_keys, preferred_element_type=j...  8.13 us
    ppermute x3, waiting for transfers between devices, hubs_find(): m_next = lax.ppermute(w2[0], 'tp', pool)  8.06 us
    dot_general x1, matrix products, attend_block(): jnp.einsum('sngqk,ksnd->qsngd', ctx_weights, ctx_values, preferred_elemen...  7.97 us
  transfers between devices with their start and end apart: 7, of which 4 were waited for; matrix products, arithmetic and copies ran while one was open for 17% of the time, Pallas kernels for 0%

profile of v1, /device:TPU:0, one launch (start us, length us, event | category | flops | bytes accessed | tf_op | source)
XLA Modules:
  0.0 219.0 jit_solution(10427119929308640314)
XLA Ops:
  6.5 1.4 fusion.51
  7.9 1.3 fusion.53
  9.2 1.3 fusion.55
  10.5 21.3 %all-reduce = (f32[3,512]{1,0:T(4,128)S(1)}, f32[3,512]{1,0:T(4,128)S(1)}, f32[3,512]{1,0:T(4,128)}) all-reduce(f32[3,512]{1,0:T(4,128)S(1)} %fusion.51, f32[3,512]{1,0:T(4,128)S(1)} %fusion.53, f32[3,512]{1,0:T(4,128)S(1)} %fusion.55), channel_id=1, replica_groups=mesh['grp'=2,'sp'=4,'tp'=4] {'sp'}, use_global_device_ids=true, to_apply=%region_3.4 | all-reduce | flops 4608 | bytes 36864 | tf_op jit(solution)/shard_map/psum | solution.py:100
  31.7 5.2 %all_gather.14 = f32[3,2048]{1,0:T(4,128)S(1)} all-gather(f32[3,512]{1,0:T(4,128)S(1)} %get-tuple-element.19), channel_id=1, replica_groups=mesh['grp'=2,'sp'=4,'tp'=4] {'tp'}, dimensions={1}, use_global_device_ids=true | all-gather | bytes 30720 | tf_op jit(solution)/shard_map/all_gather | solution.py:102
  36.9 5.2 %all_gather.13 = f32[3,2048]{1,0:T(4,128)S(1)} all-gather(f32[3,512]{1,0:T(4,128)S(1)} %get-tuple-element.20), channel_id=1, replica_groups=mesh['grp'=2,'sp'=4,'tp'=4] {'tp'}, dimensions={1}, use_global_device_ids=true | all-gather | bytes 30720 | tf_op jit(solution)/shard_map/all_gather | solution.py:103
  42.1 1.6 fusion.13
  43.7 2.8 %fusion.17 = bf16[128,2,2048]{2,0,1:T(8,128)(2,1)} fusion(f32[2,2048]{1,0:T(2,128)S(1)} %slice.77, f32[2,2048]{1,0:T(2,128)S(1)} %slice_add_fusion, f32[2048]{0:T(1024)} %param.20, f32[128,2]{0,1:T(2,128)S(1)} %add_rsqrt_fusion.1, bf16[128,2,2048]{2,1,0:T(2,128)(2,1)} %param.13), kind=kLoop, calls=%fused_computation.29 | loop fusion | flops 3145728 | bytes 2139136 | tf_op jit(solution)/shard_map/convert_element_type | solution.py:65
  46.6 0.4 collective-permute-start
  46.9 2.2 %fusion.6 = f32[256,2]{1,0:T(8,128)S(1)} fusion(bf16[256,2,2048]{2,1,0:T(2,128)(2,1)S(1)} %copy-done.4), kind=kLoop, calls=%fused_computation.14 | loop fusion | flops 3145216 | bytes 2099200 | tf_op jit(solution)/shard_map/reduce_sum | solution.py:64
  49.2 4.6 %fusion.10 = bf16[256,2,2048]{2,1,0:T(2,128)(2,1)} fusion(bf16[256,2,2048]{2,1,0:T(2,128)(2,1)S(1)} %copy-done.4, f32[2048]{0:T(1024)S(1)} %bitcast.81, f32[2048]{0:T(1024)S(1)} %bitcast.80, f32[2048]{0:T(1024)S(1)} %copy-done.15, f32[256,2]{1,0:T(8,128)S(1)} %add_rsqrt_fusion), kind=kLoop, calls=%fused_computation.18 | loop fusion | flops 6291456 | bytes 4220928 | tf_op jit(solution)/shard_map/convert_element_type | solution.py:65
  53.8 4.1 %reshape.218 = bf16[512,2048]{1,0:T(8,128)(2,1)} reshape(bf16[256,2,2048]{2,1,0:T(2,128)(2,1)} %fusion.10) | data formatting | bytes 4194304 | tf_op jit(solution)/shard_map/reshape | solution.py:138
  57.9 3.2 %collective-permute-done = bf16[128,2,2048]{2,0,1:T(8,128)(2,1)} collective-permute-done((bf16[128,2,2048]{2,0,1:T(8,128)(2,1)}, bf16[128,2,2048]{2,0,1:T(8,128)(2,1)}, u32[]{:S(2)}, u32[]{:S(2)}) %collective-permute-start) | collective-permute-done | bytes 1048608 | tf_op jit(solution)/shard_map/ppermute | solution.py:21
  61.1 2.5 %convolution_convert_fusion.1 = bf16[512,256]{1,0:T(8,128)(2,1)S(1)} fusion(bf16[512,2048]{1,0:T(8,128)(2,1)} %reshape.218, bf16[2048,128]{1,0:T(8,128)(2,1)} %param.23, bf16[2048,128]{1,0:T(8,128)(2,1)} %param.22), kind=kOutput, calls=%fused_computation.43 | convolution fusion | flops 539099136 | bytes 3407872 | tf_op jit(solution)/shard_map/dot_general | solution.py:140
  63.7 0.8 reshape.219
  64.4 0.0 all-gather.2.cloned.1.call-update
  64.5 0.0 reduce-scatter.2.cloned.1.call-start
  64.5 2.0 copy.60
  66.6 2.0 copy.59
  68.6 1.4 copy.58
  70.0 0.6 max.33
  70.7 4.9 %collective-permute-done.1 = bf16[128,2,2048]{2,0,1:T(8,128)(2,1)S(1)} collective-permute-done((bf16[128,2,2048]{2,0,1:T(8,128)(2,1)}, bf16[128,2,2048]{2,0,1:T(8,128)(2,1)S(1)}, u32[]{:S(2)}, u32[]{:S(2)}) %collective-permute-start.1) | collective-permute-done | bytes 1048608 | tf_op jit(solution)/shard_map/ppermute | solution.py:21
  75.6 0.1 broadcast_multiply_fusion.1
  75.6 0.9 fusion.34
  76.5 0.7 fusion.24
  77.3 13.8 %all-gather.2.cloned.1.call-done = bf16[1024,2,256]{2,1,0:T(2,128)(2,1)} async-done(((bf16[256,2,256]{2,1,0:T(2,128)(2,1)}), bf16[1024,2,256]{2,1,0:T(2,128)(2,1)}) %all-gather.2.cloned.1.call-update) | async-done | bytes 1048592 | tf_op jit(solution)/shard_map/all_gather | solution.py:139
  91.1 2.9 %fusion.57 = (bf16[1024,2,128]{2,1,0:T(2,128)(2,1)}, bf16[1024,2,128]{2,1,0:T(2,128)(2,1)}) fusion(bf16[1024,2,256]{2,1,0:T(2,128)(2,1)} %all-gather.2.cloned.1.call-done), kind=kLoop, calls=%fused_computation.108 | loop fusion | bytes 2097152 | tf_op jit(solution)/shard_map/slice | solution.py:148
  94.0 2.1 copy.65
  96.2 2.0 copy.63
  98.2 1.3 constant_dynamic-update-slice_fusion.7
  99.5 0.1 constant_dynamic-update-slice_fusion.6
  99.6 1.3 constant_dynamic-update-slice_fusion.5
  101.0 0.6 constant_dynamic-update-slice_fusion.4
  101.6 1.4 constant_dynamic-update-slice_fusion.3
  103.1 0.1 constant_dynamic-update-slice_fusion.2
  103.2 1.3 constant_dynamic-update-slice_fusion.1
  104.5 0.6 constant_dynamic-update-slice_fusion
  105.1 2.4 %fusion.11 = f32[512,2,512]{0,2,1:T(8,128)S(1)} fusion(bf16[1024,2,2048]{2,0,1:T(8,128)(2,1)S(1)} %constant_dynamic-update-slice_fusion, s32[]{:T(128)S(6)} %select_n.38, bf16[2048,128]{0,1:T(8,128)(2,1)S(1)} %copy-done.10, bf16[2048,128]{0,1:T(8,128)(2,1)S(1)} %copy-done.11, bf16[2048,256]{0,1:T(8,128)(2,1)S(1)} %copy-done.7), kind=kOutput, calls=%fused_computation.19 | convolution fusion | flops 2153775104 | bytes 8388612 | tf_op jit(solution)/shard_map/dot_general | solution.py:111
  107.5 0.1 slice.84
  107.7 0.2 subtract_convert_fusion
  107.9 0.1 subtract_convert_fusion.1
  108.1 1.3 collective-permute-start.4
  109.4 4.8 %collective-permute-start.3 = (bf16[128,2,256]{0,2,1:T(8,128)(2,1)S(1)}, bf16[128,2,256]{0,2,1:T(8,128)(2,1)S(1)}, u32[]{:S(2)}, u32[]{:S(2)}) collective-permute-start(bf16[128,2,256]{0,2,1:T(8,128)(2,1)S(1)} %get-tuple-element.40), channel_id=1, source_target_pairs={{0,4},{4,8},{8,12},{1,5},{5,9},{9,13},{2,6},{6,10},{10,14},{3,7},{... | collective-permute-start | bytes 393224 | tf_op jit(solution)/shard_map/ppermute | solution.py:38
  114.2 8.1 %bitcast_reduce_fusion = (f32[2,2,2,512]{3,2,1,0:T(2,128)S(1)}, f32[2,2,1024,512,2]{3,2,4,1,0:T(8,128)}) fusion(bf16[1024,2,2,64,1]{0,3,4,2,1:T(8,128)(2,1)S(1)} %bitcast.71, bf16[512,2,2,2,32]{0,4,3,2,1:T(8,128)(2,1)S(1)} %bitcast.75, bf16[512,2,2,2,32]{0,4,3,2,1:T(8,128)(2,1)S(1)} %bitcast.73), kind=kOutput, calls=%fused_computation.1 | convolution fusion | flops 546304000 | bytes 17842176 | tf_op jit(solution)/shard_map/while/body/eval_jaxpr/qsngd,ksnd->sngqk/dot_general | solution.py:178
  122.3 0.1 pad_maximum_fusion
  122.4 0.1 fusion.58
  122.5 2.1 fusion.3
  124.6 0.1 maximum_maximum_fusion
  124.7 2.6 %fusion.2 = f32[2,2,2,512]{3,2,1,0:T(2,128)S(1)} fusion(f32[2,2,768,512,2]{3,2,4,1,0:T(8,128)S(1)} %get-tuple-element.47, f32[2,2,2,512]{3,2,1,0:T(2,128)S(1)} %maximum_maximum_fusion, pred[512,768]{0,1:T(8,128)(4,1)S(1)} %fusion.24), kind=kLoop, calls=%fused_computation.8 | loop fusion | flops 12578816 | bytes 13008896 | tf_op jit(solution)/shard_map/while/body/eval_jaxpr/reduce_sum | solution.py:187
  127.3 1.9 copy-done.2
  129.1 8.6 %fusion.1 = f32[2,2,2,512]{3,2,1,0:T(2,128)S(1)} fusion(f32[2,2,1024,512,2]{3,2,4,1,0:T(8,128)} %get-tuple-element.49, f32[2,2,2,512]{3,2,1,0:T(2,128)S(1)} %maximum_maximum_fusion), kind=kLoop, calls=%fused_computation.4 | loop fusion | flops 12578816 | bytes 16809984 | tf_op jit(solution)/shard_map/while/body/eval_jaxpr/reduce_sum | solution.py:187
  137.7 0.1 exponential_add_fusion
  137.9 8.0 %fusion.4 = f32[2,2,64,2,512]{4,2,3,1,0:T(8,128)S(1)} fusion(bf16[1024,2,2,64,1]{0,3,4,2,1:T(8,128)(2,1)S(1)} %bitcast.77, f32[2,2,1024,512,2]{3,2,4,1,0:T(8,128)} %get-tuple-element.49, f32[2,2,2,512]{3,2,1,0:T(2,128)S(1)} %exponential_add_fusion, f32[2,2,2,512]{3,2,1,0:T(2,128)S(1)} %maximum_maximum_fusion), kind=kOutput, calls=%fused_computation.10 | convolution fusion | flops 553648128 | bytes 18382848 | tf_op jit(solution)/shard_map/while/body/eval_jaxpr/sngqk,ksnd->qsngd/dot_general | solution.py:194
  145.8 1.4 copy-done.3
  147.2 4.3 %fusion.27 = bf16[512,2,2,2,64]{0,4,3,2,1:T(8,128)(2,1)} fusion(f32[2,2,64,2,512]{4,2,3,1,0:T(8,128)S(1)} %fusion.4, bf16[768,2,2,64,1]{0,3,4,2,1:T(8,128)(2,1)S(1)} %bitcast.78, f32[2,2,768,512,2]{3,2,4,1,0:T(8,128)S(1)} %copy-done.3, f32[2,2,2,512]{3,2,1,0:T(2,128)S(1)} %exponential_add_fusion, f32[2,2,2,512]{3,2,1,0:T(2,128)S(1)} %maximum_maximum_fusion, ...), kind=kOutput, calls=%fused_computation.42 | convolution fusion | flops 418906112 | bytes 14974976 | tf_op jit(solution)/shard_map/while/body/eval_jaxpr/sngqk,ksnd->qsngd/dot_general | solution.py:191
  151.5 2.4 %copy.67 = bf16[512,2,2,2,64]{4,3,2,1,0:T(2,128)(2,1)S(1)} copy(bf16[512,2,2,2,64]{0,4,3,2,1:T(8,128)(2,1)} %fusion.27) | data formatting | bytes 1048576 | tf_op jit(solution)/shard_map/while/body/eval_jaxpr/convert_element_type | solution.py:197
  153.9 1.5 reshape.222
  155.4 4.3 %convolution_convert_fusion = bf16[1024,2048]{1,0:T(8,128)(2,1)} fusion(bf16[1024,256]{1,0:T(8,128)(2,1)} %reshape.222, bf16[256,2048]{1,0:T(8,128)(2,1)S(1)} %copy-done), kind=kOutput, calls=%fused_computation.21 | convolution fusion | flops 1075838976 | bytes 5767168 | tf_op jit(solution)/shard_map/dot_general | solution.py:201
  159.6 0.0 reduce-scatter.2.cloned.1.call-update
  159.7 5.2 %all_gather.12 = f32[3,2048]{1,0:T(4,128)S(1)} all-gather(f32[3,512]{1,0:T(4,128)S(1)} %copy-done.19), channel_id=1, replica_groups=mesh['grp'=2,'sp'=4,'tp'=4] {'tp'}, dimensions={1}, use_global_device_ids=true | all-gather | bytes 30720 | tf_op jit(solution)/shard_map/all_gather | solution.py:104
  164.9 38.9 %reduce-scatter.2.cloned.1.call-done = bf16[256,2048]{1,0:T(8,128)(2,1)} async-done(((bf16[1024,2048]{1,0:T(8,128)(2,1)}), bf16[256,2048]{1,0:T(8,128)(2,1)}) %reduce-scatter.2.cloned.1.call-update) | async-done | bytes 1048592 | tf_op jit(solution)/shard_map/reduce_scatter | solution.py:200
  203.7 3.3 %reshape.226 = f32[128,2,2048]{2,1,0:T(2,128)} reshape(bf16[256,2048]{1,0:T(8,128)(2,1)} %reduce-scatter.2.cloned.1.call-done) | data formatting | bytes 3145728 | tf_op jit(solution)/shard_map/reshape | solution.py:206
  207.1 3.0 %fusion.18 = bf16[128,2,2048]{2,0,1:T(8,128)(2,1)S(1)} fusion(f32[128,2,2048]{2,1,0:T(2,128)} %reshape.226, f32[2,2048]{1,0:T(2,128)S(1)} %slice.75, bf16[128,2,2048]{2,1,0:T(2,128)(2,1)S(1)} %copy-done.1), kind=kLoop, calls=%fused_computation.30 | loop fusion | flops 2097152 | bytes 4210688 | tf_op jit(solution)/shard_map/convert_element_type | solution.py:208
  210.1 2.0 copy.69
  (64 shorter events, 0.4 us)
Async XLA Ops:
  6.5 148.8 %copy-start = (bf16[256,2048]{1,0:T(8,128)(2,1)S(1)}, bf16[256,2048]{1,0:T(8,128)(2,1)}, u32[]{:S(2)}) copy-start(bf16[256,2048]{1,0:T(8,128)(2,1)} %param.25) | copy-start | bytes 3145732
  6.5 42.7 %copy-start.15 = (f32[2048]{0:T(1024)S(1)}, f32[2048]{0:T(1024)}, u32[]{:S(2)}) copy-start(f32[2048]{0:T(1024)} %param.20) | copy-start | bytes 24580
  6.5 40.4 %copy-start.4 = (bf16[256,2,2048]{2,1,0:T(2,128)(2,1)S(1)}, bf16[256,2,2048]{2,1,0:T(2,128)(2,1)}, u32[]{:S(2)}) copy-start(bf16[256,2,2048]{2,1,0:T(2,128)(2,1)} %param.14) | copy-start | bytes 6291460
  6.5 84.6 %all-gather.2.cloned.1.call-start = ((), (), s32[]{:S(2)}) async-start(), calls=%async_computation.1 | async-start | bytes 1310720 | tf_op jit(solution)/shard_map/all_gather | solution.py:139
  42.1 11.7 %copy-start.13 = (f32[2,2048]{1,0:T(2,128)}, f32[2,2048]{1,0:T(2,128)S(1)}, u32[]{:S(2)}) copy-start(f32[2,2048]{1,0:T(2,128)S(1)} %slice_add_fusion) | copy-start | bytes 49156
  43.7 3.2 %copy-start.17 = (f32[128,2]{0,1:T(2,128)}, f32[128,2]{0,1:T(2,128)S(1)}, u32[]{:S(2)}) copy-start(f32[128,2]{0,1:T(2,128)S(1)} %add_rsqrt_fusion.1) | copy-start | bytes 3076
  46.6 14.5 %collective-permute-start = (bf16[128,2,2048]{2,0,1:T(8,128)(2,1)}, bf16[128,2,2048]{2,0,1:T(8,128)(2,1)}, u32[]{:S(2)}, u32[]{:S(2)}) collective-permute-start(bf16[128,2,2048]{2,0,1:T(8,128)(2,1)} %fusion.17), channel_id=1, source_target_pairs={{0,1},{1,2},{2,3},{3,0},{4,5},{5,6},{6,7},{7,4},{8,9},{9,10},{10,1... | collective-permute-start | bytes 3145736 | tf_op jit(solution)/shard_map/ppermute | solution.py:21
  57.9 10.7 %copy-start.6 = (bf16[2048,256]{1,0:T(8,128)(2,1)S(1)}, bf16[2048,256]{1,0:T(8,128)(2,1)}, u32[]{:S(2)}) copy-start(bf16[2048,256]{1,0:T(8,128)(2,1)} %param.21) | copy-start | bytes 3145732
  57.9 12.1 %copy-start.21 = (f32[4]{0:T(128)S(1)}, f32[4]{0:T(128)}, u32[]{:S(2)}) copy-start(f32[4]{0:T(128)} %param.24) | copy-start | bytes 52
  61.1 14.4 %collective-permute-start.1 = (bf16[128,2,2048]{2,0,1:T(8,128)(2,1)}, bf16[128,2,2048]{2,0,1:T(8,128)(2,1)S(1)}, u32[]{:S(2)}, u32[]{:S(2)}) collective-permute-start(bf16[128,2,2048]{2,0,1:T(8,128)(2,1)} %collective-permute-done), channel_id=1, source_target_pairs={{0,1},{1,2},{2,3},{3,0},{4,5},{5,6},{6,7},{7,4},{8,9},{9,10},{10,1... | collective-permute-start | bytes 3145736 | tf_op jit(solution)/shard_map/ppermute | solution.py:21
  64.5 139.3 %reduce-scatter.2.cloned.1.call-start = ((), (), s32[]{:S(2)}) async-start(), calls=%async_computation.2 | async-start | bytes 5242880 | tf_op jit(solution)/shard_map/reduce_scatter | solution.py:200
  75.5 22.7 %collective-permute-start.2 = (bf16[128,2,2048]{2,0,1:T(8,128)(2,1)S(1)}, bf16[128,2,2048]{2,0,1:T(8,128)(2,1)}, u32[]{:S(2)}, u32[]{:S(2)}) collective-permute-start(bf16[128,2,2048]{2,0,1:T(8,128)(2,1)S(1)} %collective-permute-done.1), channel_id=1, source_target_pairs={{0,1},{1,2},{2,3},{3,0},{4,5},{5,6},{6,7},{7,4},{8,9},{9,10},{10,1... | collective-permute-start | bytes 3145736 | tf_op jit(solution)/shard_map/ppermute | solution.py:21
  94.0 6.9 %copy-start.1 = (bf16[128,2,2048]{2,1,0:T(2,128)(2,1)S(1)}, bf16[128,2,2048]{2,1,0:T(2,128)(2,1)}, u32[]{:S(2)}) copy-start(bf16[128,2,2048]{2,1,0:T(2,128)(2,1)} %param.13) | copy-start | bytes 3145732
  98.2 2.8 %copy-start.14 = (f32[2,2048]{1,0:T(2,128)S(1)}, f32[2,2048]{1,0:T(2,128)}, u32[]{:S(2)}) copy-start(f32[2,2048]{1,0:T(2,128)} %copy-done.13) | copy-start | bytes 49156
  98.2 2.8 %copy-start.16 = (f32[2048]{0:T(1024)S(1)}, f32[2048]{0:T(1024)}, u32[]{:S(2)}) copy-start(f32[2048]{0:T(1024)} %param.20) | copy-start | bytes 24580
  98.2 2.8 %copy-start.18 = (f32[128,2]{0,1:T(2,128)S(1)}, f32[128,2]{0,1:T(2,128)}, u32[]{:S(2)}) copy-start(f32[128,2]{0,1:T(2,128)} %copy-done.17) | copy-start | bytes 3076
  101.6 3.5 %copy-start.7 = (bf16[2048,256]{0,1:T(8,128)(2,1)S(1)}, bf16[2048,256]{0,1:T(8,128)(2,1)}, u32[]{:S(2)}) copy-start(bf16[2048,256]{0,1:T(8,128)(2,1)} %copy.58) | copy-start | bytes 3145732
  101.6 3.5 %copy-start.10 = (bf16[2048,128]{0,1:T(8,128)(2,1)S(1)}, bf16[2048,128]{0,1:T(8,128)(2,1)}, u32[]{:S(2)}) copy-start(bf16[2048,128]{0,1:T(8,128)(2,1)} %copy.60) | copy-start | bytes 1572868
  101.6 3.5 %copy-start.11 = (bf16[2048,128]{0,1:T(8,128)(2,1)S(1)}, bf16[2048,128]{0,1:T(8,128)(2,1)}, u32[]{:S(2)}) copy-start(bf16[2048,128]{0,1:T(8,128)(2,1)} %copy.59) | copy-start | bytes 1572868
  105.1 2.6 %copy-start.8 = (f32[512,32]{0,1:T(8,128)S(1)}, f32[512,32]{0,1:T(8,128)}, u32[]{:S(2)}) copy-start(f32[512,32]{0,1:T(8,128)} %get-tuple-element.42) | copy-start | bytes 196612
  105.1 2.6 %copy-start.9 = (f32[512,32]{0,1:T(8,128)S(1)}, f32[512,32]{0,1:T(8,128)}, u32[]{:S(2)}) copy-start(f32[512,32]{0,1:T(8,128)} %get-tuple-element.43) | copy-start | bytes 196612
  107.5 6.6 %copy-start.5 = (bf16[1024,2,128]{0,2,1:T(8,128)(2,1)S(1)}, bf16[1024,2,128]{0,2,1:T(8,128)(2,1)}, u32[]{:S(2)}) copy-start(bf16[1024,2,128]{0,2,1:T(8,128)(2,1)} %copy.63) | copy-start | bytes 1572868
  108.1 14.2 %collective-permute-start.4 = (bf16[128,2,256]{0,2,1:T(8,128)(2,1)S(1)}, bf16[128,2,256]{0,2,1:T(8,128)(2,1)S(1)}, u32[]{:S(2)}, u32[]{:S(2)}) collective-permute-start(bf16[128,2,256]{0,2,1:T(8,128)(2,1)S(1)} %get-tuple-element.41), channel_id=1, source_target_pairs={{4,0},{8,4},{12,8},{5,1},{9,5},{13,9},{6,2},{10,6},{14,10},{7,3},{... | collective-permute-start | bytes 393224 | tf_op jit(solution)/shard_map/ppermute | solution.py:40
  109.4 12.9 %collective-permute-start.3 = (bf16[128,2,256]{0,2,1:T(8,128)(2,1)S(1)}, bf16[128,2,256]{0,2,1:T(8,128)(2,1)S(1)}, u32[]{:S(2)}, u32[]{:S(2)}) collective-permute-start(bf16[128,2,256]{0,2,1:T(8,128)(2,1)S(1)} %get-tuple-element.40), channel_id=1, source_target_pairs={{0,4},{4,8},{8,12},{1,5},{5,9},{9,13},{2,6},{6,10},{10,14},{3,7},{... | collective-permute-start | bytes 393224 | tf_op jit(solution)/shard_map/ppermute | solution.py:38
  122.4 2.2 copy-start.20
  124.6 4.5 %copy-start.2 = (f32[2,2,768,512,2]{3,2,4,1,0:T(8,128)}, f32[2,2,768,512,2]{3,2,4,1,0:T(8,128)S(1)}, u32[]{:S(2)}) copy-start(f32[2,2,768,512,2]{3,2,4,1,0:T(8,128)S(1)} %get-tuple-element.47) | copy-start | bytes 37748740
  129.1 8.7 %copy-start.12 = (bf16[1024,2,128]{0,2,1:T(8,128)(2,1)S(1)}, bf16[1024,2,128]{0,2,1:T(8,128)(2,1)}, u32[]{:S(2)}) copy-start(bf16[1024,2,128]{0,2,1:T(8,128)(2,1)} %copy.65) | copy-start | bytes 1572868
  137.8 9.3 %copy-start.3 = (f32[2,2,768,512,2]{3,2,4,1,0:T(8,128)S(1)}, f32[2,2,768,512,2]{3,2,4,1,0:T(8,128)}, u32[]{:S(2)}) copy-start(f32[2,2,768,512,2]{3,2,4,1,0:T(8,128)} %copy-done.2) | copy-start | bytes 37748740
  155.4 4.3 %copy-start.19 = (f32[3,512]{1,0:T(4,128)S(1)}, f32[3,512]{1,0:T(4,128)}, u32[]{:S(2)}) copy-start(f32[3,512]{1,0:T(4,128)} %get-tuple-element.21) | copy-start | bytes 18436
Sparse Core Ops, SparseCore 0:
  64.6 26.5 all-gather.1
  159.8 43.9 reduce-scatter.1
